TPU v7x, 32 devices: a whole 2x2x4 slice. The times are simulated.
32 devices in a mesh: ep: 8 (over z, core), tp: 4 (over y, x).
Axes of the slice: x: 2, y: 2, z: 4, core: 2. Of those that a mesh axis runs over, the one named last changes fastest.
Arguments:
- mixer_rows: bfloat16 [4096, 2048], P('ep', 'tp'), may hold values from -6 to 6
- expert_rows: bfloat16 [4096, 2048], P('ep', 'tp'), may hold values from -6 to 6
- mixer_gain: float32 [2048], replicated, may hold values from 0.1 to 1.9
- pool_scale: float32 [2048], P('tp'), may hold values from 0.1 to 1.9
- w_in: bfloat16 [2048, 2048], P(None, 'tp'), may hold values from -0.125 to 0.125
- w_mix_out: bfloat16 [2048, 2048], P(None, 'tp'), may hold values from -0.125 to 0.125
- expert_gain: float32 [2048], replicated, may hold values from 0.1 to 1.9
- expert_gate: bfloat16 [8, 2048, 2048], P('ep', None, 'tp'), may hold values from -0.125 to 0.125
- expert_up: bfloat16 [8, 2048, 2048], P('ep', None, 'tp'), may hold values from -0.125 to 0.125
- expert_down: bfloat16 [8, 2048, 2048], P('ep', None, 'tp'), may hold values from -0.125 to 0.125
- routes: int32 [4096, 2], P('ep'), may hold values from 0 to 7, all different within a row; in each aligned block of 512 rows (0 to 511, 512 to 1023, ...) at most 192 rows name the same one
- route_weight: float32 [4096, 2], P('ep'), may hold values from 0.1 to 1
Outputs:
- mixer_output: bfloat16 [4096, 2048], P('ep', 'tp')
- expert_output: bfloat16 [4096, 2048], P('ep', 'tp')
Inputs may be any that keep to these rules, and one draw needn't show every extreme that they name: `routes`: each row names 2 different experts. Among the rows of one device (aligned blocks of 512 rows) no expert is named more than 192 times, a bound that some block reaches.
All inputs are finite; a program needn't handle non-finite values.
Results may differ from a plain program's by a relative error of at most 0.0071.
Values may be sent and summed in bfloat16 or wider, within the bound.
No kernel may reach another device: no remote copies, remote signals or barrier semaphores. Data moves between devices by JAX's collectives and lax.ppermute only.
A program may use at most 64 MiB of HBM per device.

v0:
```python
import jax
import jax.numpy as jnp
from jax import lax
from jax.sharding import PartitionSpec as P

PW = 2048
TOP = 2
norm_eps = 1e-05
pool_windows = (2, 4, 8, 16)
rim_rows = 8


def extended_2(block, sides, width):
    for axis, dim in sides:
        count = lax.axis_size(axis)
        forward = [(i, i + 1) for i in range(count - 1)]
        backward = [(target, source) for source, target in forward]
        low = lax.ppermute(
            lax.slice_in_dim(block, block.shape[dim] - width, None, axis=dim), axis, forward
        )
        high = lax.ppermute(lax.slice_in_dim(block, 0, width, axis=dim), axis, backward)
        block = jnp.concatenate([low, block, high], axis=dim)
    return block


def layer_norm(row_block, gain_vec):
    values = row_block.astype(jnp.float32)
    center = values - jnp.mean(values, axis=-1, keepdims=True)
    spread = jnp.mean(center * center, axis=-1, keepdims=True)
    return (center * lax.rsqrt(spread + norm_eps) * gain_vec).astype(jnp.bfloat16)


def pooled_channels(inner_t, scale_local, ep_size, ep_index, tp_index):
    extended = extended_2(inner_t, (("ep", 1),), rim_rows).astype(jnp.float32)
    values = inner_t.astype(jnp.float32)
    channels = values.shape[0]
    row_count = values.shape[1]
    seq_len = row_count * ep_size
    position = ep_index * row_count + jnp.arange(row_count, dtype=jnp.int32)
    channel = tp_index * channels + jnp.arange(channels, dtype=jnp.int32)
    group = channel // (PW // 4)
    running = jnp.zeros((channels, row_count), jnp.float32)
    result = jnp.zeros((channels, row_count), jnp.float32)
    last_half = 0
    for group_id, window in enumerate(pool_windows):
        half_span = window // 2
        for offset in list(range(-half_span, -last_half)) + list(range(last_half, half_span)):
            running = running + extended[:, rim_rows + offset : rim_rows + offset + row_count]
        last_half = half_span
        lower_end = jnp.clip(position - half_span, 0, seq_len)
        upper_end = jnp.clip(position - half_span + window, 0, seq_len)
        counts = (upper_end - lower_end).astype(jnp.float32)
        member = (group == group_id)[:, None]
        result = jnp.where(member, running / counts[None, :], result)
    return ((result - values) * scale_local[:, None]).astype(jnp.bfloat16)


def on_device(
    mixer_rows,
    expert_rows,
    mixer_gain,
    pool_scale,
    w_in,
    w_mix_out,
    expert_gain,
    expert_gate,
    expert_up,
    expert_down,
    routes,
    route_weight,
):
    ep_size = lax.axis_size("ep")
    ep_index = lax.axis_index("ep")
    tp_index = lax.axis_index("tp")
    row_count = routes.shape[0]
    capacity = (3 * TOP * row_count + 2 * ep_size - 1) // (2 * ep_size)
    flat_route = routes.reshape(-1)
    onehot = (flat_route[:, None] == jnp.arange(ep_size, dtype=jnp.int32)[None, :]).astype(
        jnp.int32
    )
    ranking = jnp.sum(onehot * (jnp.cumsum(onehot, axis=0) - 1), axis=1)
    target = flat_route * capacity + ranking
    sender = (
        jnp.zeros((ep_size * capacity,), jnp.int32)
        .at[target]
        .set(jnp.arange(row_count * TOP, dtype=jnp.int32) // TOP + 1)
    )
    filled = (sender > 0)[:, None]
    source_row = jnp.maximum(sender - 1, 0)
    full_mix = lax.all_gather(mixer_rows, "tp", axis=1, tiled=True)
    feature_count = expert_rows.shape[1]
    outgoing = jnp.where(filled, expert_rows[source_row], jnp.zeros((), jnp.bfloat16))
    arrived = lax.all_to_all(
        outgoing.reshape(ep_size, capacity, feature_count),
        "ep",
        split_axis=0,
        concat_axis=0,
        tiled=True,
    )
    slot_slices = arrived.reshape(ep_size * capacity, feature_count)
    slot_normed = layer_norm(lax.all_gather(slot_slices, "tp", axis=1, tiled=True), expert_gain)
    contract_first = (((0,), (1,)), ((), ()))
    normed_mix = layer_norm(full_mix, mixer_gain)
    inner_t = lax.dot_general(
        w_in, normed_mix, contract_first, preferred_element_type=jnp.float32
    ).astype(jnp.bfloat16)
    pooled_t = pooled_channels(inner_t, pool_scale, ep_size, ep_index, tp_index)
    gate_t = lax.dot_general(
        expert_gate[0], slot_normed, contract_first, preferred_element_type=jnp.float32
    )
    up_t = lax.dot_general(
        expert_up[0], slot_normed, contract_first, preferred_element_type=jnp.float32
    )
    hidden_t = (jax.nn.silu(gate_t) * up_t).astype(jnp.bfloat16)
    contract_lead = (((0,), (0,)), ((), ()))
    down_weight = expert_down[0]
    mixed_sum = lax.dot_general(
        lax.all_gather(pooled_t, "tp", axis=0, tiled=True),
        w_mix_out,
        contract_lead,
        preferred_element_type=jnp.float32,
    )
    expert_sum = lax.dot_general(
        lax.all_gather(hidden_t, "tp", axis=0, tiled=True),
        down_weight,
        contract_lead,
        preferred_element_type=jnp.float32,
    )
    mixer_output = mixed_sum.astype(jnp.bfloat16)
    back_rows = expert_sum.astype(jnp.bfloat16).reshape(ep_size, capacity, expert_sum.shape[1])
    returned = lax.all_to_all(back_rows, "ep", split_axis=0, concat_axis=0, tiled=True).reshape(
        ep_size * capacity, expert_sum.shape[1]
    )
    picked = returned[target].astype(jnp.float32).reshape(row_count, TOP, expert_sum.shape[1])
    expert_output = jnp.sum(picked * route_weight[:, :, None], axis=1).astype(jnp.bfloat16)
    return (mixer_output, expert_output)


def solution(mesh):
    return jax.shard_map(
        on_device,
        mesh=mesh,
        in_specs=(
            P("ep", "tp"),
            P("ep", "tp"),
            P(),
            P("tp"),
            P(None, "tp"),
            P(None, "tp"),
            P(),
            P("ep", None, "tp"),
            P("ep", None, "tp"),
            P("ep", None, "tp"),
            P("ep", None),
            P("ep", None),
        ),
        out_specs=(P("ep", "tp"), P("ep", "tp")),
        check_vma=False,
    )
```

profile of v0, /device:TPU:0, one launch (start us, length us, event | category | flops | bytes accessed | tf_op | source)
XLA Modules:
  0.0 316.2 jit_solution(4581051959690600166)
XLA Ops:
  7.2 1.0 copy.16
  8.6 0.7 broadcast_multiply_fusion.1
  9.3 2.3 reduce-window.6
  12.5 4.3 %scatter_custom_fusion = s32[1536]{0:T(1024)S(1)} fusion(s32[1024]{0:T(1024)S(1)} %bitcast.50, s32[1024]{0:T(1024)S(1)} %fusion.34, s32[]{:T(128)} %constant.78.clone.1), kind=kCustom, calls=%fused_computation.76 | custom fusion | bytes 6148 | tf_op jit(solution)/shard_map/scatter | solution.py:86
  16.9 5.4 %gather_fusion = bf16[1536,512]{1,0:T(8,128)(2,1)} fusion(bf16[512,512]{1,0:T(8,128)(2,1)S(1)} %copy-done.1, s32[2048]{0:T(1024)S(1)} %pad_clamp_fusion), kind=kCustom, calls=%fused_computation | custom fusion | bytes 3151872 | tf_op jit(solution)/shard_map/gather | solution.py:92
  22.3 1.7 broadcast_select_fusion
  24.0 44.1 %all_to_all.10 = bf16[8,192,512]{2,1,0:T(8,128)(2,1)} all-to-all(bf16[8,192,512]{2,1,0:T(8,128)(2,1)S(1)} %broadcast_select_fusion), channel_id=1, replica_groups=mesh['ep'=8,'tp'=4] {'ep'}, dimensions={0} | all-to-all | bytes 3145728 | tf_op jit(solution)/shard_map/all_to_all | solution.py:93
  68.2 0.7 all-gather.5.cloned.1.call-update
  68.9 68.2 %all-gather.9.cloned.1.call-done = bf16[1536,2048]{1,0:T(8,128)(2,1)} async-done(((bf16[1536,512]{1,0:T(8,128)(2,1)}), bf16[1536,2048]{1,0:T(8,128)(2,1)}) %all-gather.9.cloned.1.call-update) | async-done | bytes 6291472 | tf_op jit(solution)/shard_map/all_gather | solution.py:101
  137.1 3.8 %convert_reduce_fusion = f32[1536]{0:T(1024)S(1)} fusion(bf16[1536,2048]{1,0:T(8,128)(2,1)} %all-gather.9.cloned.1.call-done), kind=kLoop, calls=%fused_computation.4 | loop fusion | flops 6289920 | bytes 6297600 | tf_op jit(solution)/shard_map/reduce_sum | solution.py:28
  140.9 0.8 copy-done.2
  141.7 1.8 fusion.2
  143.5 2.4 fusion.4
  146.0 3.4 %convolution_bitcast_fusion.1 = f32[512,1536]{0,1:T(8,128)S(1)} fusion(bf16[1536,2048]{1,0:T(8,128)(2,1)S(1)} %fusion.4, bf16[1,2048,512]{2,1,0:T(8,128)(2,1)S(1)} %copy-done), kind=kOutput, calls=%fused_computation.19 | convolution fusion | flops 3221225472 | bytes 11534336 | tf_op jit(solution)/shard_map/dot_general | solution.py:108
  149.4 4.8 %fusion.11 = bf16[512,1536]{0,1:T(8,128)(2,1)} fusion(bf16[1536,2048]{1,0:T(8,128)(2,1)S(1)} %fusion.4, f32[512,1536]{0,1:T(8,128)S(1)} %convolution_bitcast_fusion.1, bf16[1,2048,512]{2,1,0:T(8,128)(2,1)S(1)} %copy-done.7), kind=kOutput, calls=%fused_computation.20 | convolution fusion | flops 3225944064 | bytes 13107200 | tf_op jit(solution)/shard_map/dot_general | solution.py:111
  154.5 19.4 %all-gather.5.cloned.1.call-done = bf16[512,2048]{1,0:T(8,128)(2,1)} async-done(((bf16[512,512]{1,0:T(8,128)(2,1)}), bf16[512,2048]{1,0:T(8,128)(2,1)}) %all-gather.5.cloned.1.call-update) | async-done | bytes 2097168 | tf_op jit(solution)/shard_map/all_gather | solution.py:90
  174.0 2.1 convert_reduce_fusion.1
  176.2 0.7 fusion.7
  176.9 1.3 fusion.23
  178.3 1.6 collective-permute-start
  179.9 1.3 collective-permute-start.1
  181.2 3.2 %collective-permute-done.1 = bf16[512,8]{0,1:T(8,128)(2,1)S(1)} collective-permute-done((bf16[512,8]{0,1:T(8,128)(2,1)S(1)}, bf16[512,8]{0,1:T(8,128)(2,1)S(1)}, u32[]{:S(2)}, u32[]{:S(2)}) %collective-permute-start.1) | collective-permute-done | bytes 8224 | tf_op jit(solution)/shard_map/ppermute | solution.py:21
  184.5 3.3 %fusion.30 = bf16[512,512]{0,1:T(8,128)(2,1)} fusion(bf16[512,512]{0,1:T(8,128)(2,1)S(1)} %fusion.23, f32[512,528]{0,1:T(8,128)S(1)} %maximum_convert_fusion, f32[512]{0:T(512)S(1)} %copy-done.6, f32[512]{0:T(512)S(1)} %get-tuple-element.4, f32[512]{0:T(512)S(1)} %get-tuple-element.5, f32[512]{0:T(512)S(1)} %get-tuple-element.6, ...), kind=kLoop, calls=%fused_computation.53 | loop fusion | flops 7077888 | bytes 17838080 | tf_op jit(solution)/shard_map/convert_element_type | solution.py:55
  187.8 57.9 %all-gather.11.cloned.1.call-done = bf16[2048,1536]{0,1:T(8,128)(2,1)} async-done(((bf16[512,1536]{0,1:T(8,128)(2,1)}), bf16[2048,1536]{0,1:T(8,128)(2,1)}) %all-gather.11.cloned.1.call-update) | async-done | bytes 6291472 | tf_op jit(solution)/shard_map/all_gather | solution.py:124
  245.8 8.1 %convolution_convert_fusion = bf16[1536,512]{1,0:T(8,128)(2,1)} fusion(bf16[2048,1536]{0,1:T(8,128)(2,1)} %all-gather.11.cloned.1.call-done, bf16[1,2048,512]{2,1,0:T(8,128)(2,1)} %param.21), kind=kOutput, calls=%fused_computation.21 | convolution fusion | flops 3222011904 | bytes 9961472 | tf_op jit(solution)/shard_map/dot_general | solution.py:123
  253.8 4.7 %all-to-all-start.1 = ((bf16[8,192,512]{2,1,0:T(8,128)(2,1)}), bf16[8,192,512]{2,1,0:T(8,128)(2,1)}, u32[]{:S(2)}, u32[]{:S(2)}) async-start(bf16[8,192,512]{2,1,0:T(8,128)(2,1)} %bitcast.48), calls=%async_computation.1 | async-start | bytes 3145728 | tf_op jit(solution)/shard_map/all_to_all | solution.py:131
  258.7 24.3 %all-gather.7.cloned.1.call-done = bf16[2048,512]{0,1:T(8,128)(2,1)} async-done(((bf16[512,512]{0,1:T(8,128)(2,1)}), bf16[2048,512]{0,1:T(8,128)(2,1)}) %all-gather.7.cloned.1.call-update) | async-done | bytes 2097168 | tf_op jit(solution)/shard_map/all_gather | solution.py:118
  283.1 4.3 %convolution_convert_fusion.1 = bf16[512,512]{1,0:T(8,128)(2,1)} fusion(bf16[2048,512]{0,1:T(8,128)(2,1)} %all-gather.7.cloned.1.call-done, bf16[2048,512]{1,0:T(8,128)(2,1)} %param.17), kind=kOutput, calls=%fused_computation.32 | convolution fusion | flops 1074003968 | bytes 4718592 | tf_op jit(solution)/shard_map/dot_general | solution.py:117
  287.4 9.1 %all-to-all-done.1 = bf16[8,192,512]{2,1,0:T(8,128)(2,1)} async-done(((bf16[8,192,512]{2,1,0:T(8,128)(2,1)}), bf16[8,192,512]{2,1,0:T(8,128)(2,1)}, u32[]{:S(2)}, u32[]{:S(2)}) %all-to-all-start.1) | async-done | bytes 1572896 | tf_op jit(solution)/shard_map/all_to_all | solution.py:131
  296.5 5.6 %gather_fusion.1 = bf16[1024,512]{1,0:T(8,128)(2,1)S(1)} fusion(bf16[1536,512]{1,0:T(8,128)(2,1)} %bitcast.12, s32[1024]{0:T(1024)S(1)} %broadcast_clamp_fusion), kind=kCustom, calls=%fused_computation.1 | custom fusion | bytes 2101248 | tf_op jit(solution)/shard_map/gather | solution.py:134
  302.1 2.4 reshape.168
  304.4 5.2 %multiply_reduce_fusion = bf16[512,512]{1,0:T(8,128)(2,1)} fusion(f32[512,2,512]{2,1,0:T(2,128)} %reshape.168, f32[512,2]{1,0:T(8,128)S(1)} %copy.18), kind=kLoop, calls=%fused_computation.26 | loop fusion | flops 786432 | bytes 2625536 | tf_op jit(solution)/shard_map/reduce_sum | solution.py:135
  (54 shorter events, 2.2 us)
Async XLA Ops:
  7.2 138.8 %copy-start = (bf16[1,2048,512]{2,1,0:T(8,128)(2,1)S(1)}, bf16[1,2048,512]{2,1,0:T(8,128)(2,1)}, u32[]{:S(2)}) copy-start(bf16[1,2048,512]{2,1,0:T(8,128)(2,1)} %param.19) | copy-start | bytes 6291460
  7.2 9.8 %copy-start.1 = (bf16[512,512]{1,0:T(8,128)(2,1)S(1)}, bf16[512,512]{1,0:T(8,128)(2,1)}, u32[]{:S(2)}) copy-start(bf16[512,512]{1,0:T(8,128)(2,1)} %param.13) | copy-start | bytes 1572868
  7.2 129.9 %all-gather.9.cloned.1.call-start = ((), (), s32[]{:S(2)}) async-start(), calls=%async_computation.4 | async-start | bytes 7864320 | tf_op jit(solution)/shard_map/all_gather | solution.py:101
  68.1 105.9 %all-gather.5.cloned.1.call-start = ((), (), s32[]{:S(2)}) async-start(), calls=%async_computation.2 | async-start | bytes 2621440 | tf_op jit(solution)/shard_map/all_gather | solution.py:90
  68.9 176.9 %all-gather.11.cloned.1.call-start = ((), (), s32[]{:S(2)}) async-start(), calls=%async_computation.5 | async-start | bytes 7864320 | tf_op jit(solution)/shard_map/all_gather | solution.py:124
  137.1 4.6 %copy-start.2 = (bf16[1536,2048]{1,0:T(8,128)(2,1)S(1)}, bf16[1536,2048]{1,0:T(8,128)(2,1)}, u32[]{:S(2)}) copy-start(bf16[1536,2048]{1,0:T(8,128)(2,1)} %all-gather.9.cloned.1.call-done) | copy-start | bytes 18874372
  141.7 1.8 copy-start.4
  145.9 3.5 %copy-start.7 = (bf16[1,2048,512]{2,1,0:T(8,128)(2,1)S(1)}, bf16[1,2048,512]{2,1,0:T(8,128)(2,1)}, u32[]{:S(2)}) copy-start(bf16[1,2048,512]{2,1,0:T(8,128)(2,1)} %param.20) | copy-start | bytes 6291460
  154.3 128.8 %all-gather.7.cloned.1.call-start = ((), (), s32[]{:S(2)}) async-start(), calls=%async_computation.3 | async-start | bytes 2621440 | tf_op jit(solution)/shard_map/all_gather | solution.py:118
  174.0 2.2 copy-start.3
  174.0 2.9 copy-start.8
  174.0 2.9 copy-start.9
  176.9 7.6 %copy-start.6 = (f32[512]{0:T(512)S(1)}, f32[512]{0:T(512)}, u32[]{:S(2)}) copy-start(f32[512]{0:T(512)} %param.15) | copy-start | bytes 6148
  178.3 2.9 collective-permute-start
  179.9 4.5 %collective-permute-start.1 = (bf16[512,8]{0,1:T(8,128)(2,1)S(1)}, bf16[512,8]{0,1:T(8,128)(2,1)S(1)}, u32[]{:S(2)}, u32[]{:S(2)}) collective-permute-start(bf16[512,8]{0,1:T(8,128)(2,1)S(1)} %get-tuple-element.3), channel_id=1, source_target_pairs={{4,0},{8,4},{12,8},{16,12},{20,16},{24,20},{28,24},{5,1},{9,5},{13... | collective-permute-start | bytes 24584 | tf_op jit(solution)/shard_map/ppermute | solution.py:21
  253.8 4.7 %copy-start.5 = (f32[512,2]{0,1:T(2,128)S(1)}, f32[512,2]{0,1:T(2,128)}, u32[]{:S(2)}) copy-start(f32[512,2]{0,1:T(2,128)} %param.23) | copy-start | bytes 12292
  253.8 42.6 %all-to-all-start.1 = ((bf16[8,192,512]{2,1,0:T(8,128)(2,1)}), bf16[8,192,512]{2,1,0:T(8,128)(2,1)}, u32[]{:S(2)}, u32[]{:S(2)}) async-start(bf16[8,192,512]{2,1,0:T(8,128)(2,1)} %bitcast.48), calls=%async_computation.1 | async-start | bytes 3145728 | tf_op jit(solution)/shard_map/all_to_all | solution.py:131
Sparse Core Ops, SparseCore 0:
  68.2 68.8 all-gather.8
  138.9 35.0 all-gather.4
  175.8 69.8 all-gather.10
  248.0 35.0 all-gather.6
where the time goes:
time: 317 us; the launch traced here: 316 us
  waiting for transfers between devices  183 us (58%)
  blocking collectives  44.1 us (14%)
  other arithmetic  24.5 us (8%)
  matrix products  21.9 us (7%)
  local copies, waits for them, and re-layouts  20.8 us (7%)
  between operations  14.1 us (4%)
  starting transfers between devices  7.95 us (3%)
    all_gather x1, waiting for transfers between devices, on_device(): lax.all_gather(slot_slices, 'tp', axis=1, tiled=True)  68.2 us
    all_gather x1, waiting for transfers between devices, on_device(): lax.all_gather(hidden_t, 'tp', axis=0, tiled=True)  57.9 us
    all_to_all x1, blocking collectives, on_device(): lax.all_to_all(outgoing.reshape(ep_size, capacity, feature_count), 'ep',...  44.1 us
    all_gather x1, waiting for transfers between devices, on_device(): lax.all_gather(pooled_t, 'tp', axis=0, tiled=True)  24.3 us
    all_gather x1, waiting for transfers between devices, on_device(): full_mix = lax.all_gather(mixer_rows, 'tp', axis=1, tiled=True)  19.4 us
    all_to_all x1, waiting for transfers between devices, on_device(): lax.all_to_all(back_rows, 'ep', split_axis=0, concat_axis=0, tiled=True)  9.13 us
    dot_general x1, matrix products, on_device(): lax.dot_general(lax.all_gather(hidden_t, 'tp', axis=0, tiled=True), down_...  8.08 us
  transfers between devices with their start and end apart: 7, of which 6 were waited for; matrix products, arithmetic and copies ran while one was open for 12% of the time, Pallas kernels for 0%

commit v1 on v0

--- a/solution.py
+++ b/solution.py
@@ -98,7 +98,12 @@
         tiled=True,
     )
     slot_slices = arrived.reshape(ep_size * capacity, feature_count)
-    slot_normed = layer_norm(lax.all_gather(slot_slices, "tp", axis=1, tiled=True), expert_gain)
+    slot_normed = layer_norm(
+        jnp.concatenate(
+            lax.all_to_all(jnp.stack([slot_slices] * lax.axis_size("tp")), "tp", 0, 0), axis=1
+        ),
+        expert_gain,
+    )
     contract_first = (((0,), (1,)), ((), ()))
     normed_mix = layer_norm(full_mix, mixer_gain)
     inner_t = lax.dot_general(

time: 317 us -> 328 us (1.035)
  local copies, waits for them, and re-layouts: 20.8 us -> 27.2 us
  starting transfers between devices: 7.95 us -> 13.2 us
  waiting for transfers between devices: 183 us -> 178 us
  other arithmetic: 24.5 us -> 29.3 us
    all_to_all x0 -> x1, waiting for transfers between devices: none -> 85.7 us  [on_device(): lax.all_to_all(jnp.stack([slot_slices] * lax.axis_size('tp')), 'tp', 0, 0)]
    all_gather x1 -> x0, waiting for transfers between devices: 68.2 us -> none  [on_device(): lax.all_gather(slot_slices, 'tp', axis=1, tiled=True)]
    all_gather x1, waiting for transfers between devices: 19.4 us -> 0.02 us  [on_device(): full_mix = lax.all_gather(mixer_rows, 'tp', axis=1, tiled=True)]
    another operation x0 -> x2, local copies, waits for them, and re-layouts: none -> 7.12 us  [on_device(): jnp.stack([slot_slices] * lax.axis_size('tp'))]
    all_to_all x0 -> x1, starting transfers between devices: none -> 5.36 us  [on_device(): lax.all_to_all(jnp.stack([slot_slices] * lax.axis_size('tp')), 'tp', 0, 0)]
    another operation x2 -> x3, other arithmetic: 2.43 us -> 7.08 us
  transfers between devices with their start and end apart: 7 -> 7, of which waited for: 6 -> 5; matrix products, arithmetic and copies ran while one was open for 12% -> 13% of each run, Pallas kernels for 0% -> 0%
where the time goes in v1:
time: 328 us
  waiting for transfers between devices  178 us (54%)
  blocking collectives  44.1 us (13%)
  other arithmetic  29.3 us (9%)
  local copies, waits for them, and re-layouts  27.2 us (8%)
  matrix products  22.1 us (7%)
  between operations  14.1 us (4%)
  starting transfers between devices  13.2 us (4%)
    all_to_all x1, waiting for transfers between devices, on_device(): lax.all_to_all(jnp.stack([slot_slices] * lax.axis_size('tp')), 'tp', 0, 0)  85.7 us
    all_gather x1, waiting for transfers between devices, on_device(): lax.all_gather(hidden_t, 'tp', axis=0, tiled=True)  56.3 us
    all_to_all x1, blocking collectives, on_device(): lax.all_to_all(outgoing.reshape(ep_size, capacity, feature_count), 'ep',...  44.1 us
    all_gather x1, waiting for transfers between devices, on_device(): lax.all_gather(pooled_t, 'tp', axis=0, tiled=True)  24.5 us
    all_to_all x1, waiting for transfers between devices, on_device(): lax.all_to_all(back_rows, 'ep', split_axis=0, concat_axis=0, tiled=True)  8.98 us
    dot_general x1, matrix products, on_device(): lax.dot_general(lax.all_gather(hidden_t, 'tp', axis=0, tiled=True), down_...  8.08 us
    another operation x2, local copies, waits for them, and re-layouts, on_device(): jnp.stack([slot_slices] * lax.axis_size('tp'))  7.12 us
    another operation x3, other arithmetic  7.08 us
  transfers between devices with their start and end apart: 7, of which 5 were waited for; matrix products, arithmetic and copies ran while one was open for 13% of the time, Pallas kernels for 0%

profile of v1, /device:TPU:0, one launch (start us, length us, event | category | flops | bytes accessed | tf_op | source)
XLA Modules:
  0.0 327.6 jit_solution(9710465441719127323)
XLA Ops:
  7.2 1.0 copy.16
  8.5 0.7 broadcast_multiply_fusion.1
  9.2 2.3 reduce-window.6
  12.4 4.3 %scatter_custom_fusion = s32[1536]{0:T(1024)S(1)} fusion(s32[1024]{0:T(1024)S(1)} %bitcast.55, s32[1024]{0:T(1024)S(1)} %fusion.34, s32[]{:T(128)} %constant.78.clone.1), kind=kCustom, calls=%fused_computation.76 | custom fusion | bytes 6148 | tf_op jit(solution)/shard_map/scatter | solution.py:86
  16.9 5.4 %gather_fusion = bf16[1536,512]{1,0:T(8,128)(2,1)} fusion(bf16[512,512]{1,0:T(8,128)(2,1)S(1)} %copy-done.1, s32[2048]{0:T(1024)S(1)} %pad_clamp_fusion), kind=kCustom, calls=%fused_computation | custom fusion | bytes 3151872 | tf_op jit(solution)/shard_map/gather | solution.py:92
  22.3 1.7 broadcast_select_fusion
  24.0 44.1 %all_to_all.15 = bf16[8,192,512]{2,1,0:T(8,128)(2,1)} all-to-all(bf16[8,192,512]{2,1,0:T(8,128)(2,1)S(1)} %broadcast_select_fusion), channel_id=1, replica_groups=mesh['ep'=8,'tp'=4] {'ep'}, dimensions={0} | all-to-all | bytes 3145728 | tf_op jit(solution)/shard_map/all_to_all | solution.py:93
  68.0 2.6 copy.18
  70.6 4.5 %stack.3 = bf16[4,1536,512]{1,2,0:T(8,128)(2,1)} broadcast(bf16[1536,512]{0,1:T(8,128)(2,1)} %copy.18), dimensions={1,2} | broadcast | bytes 7864320 | tf_op jit(solution)/shard_map/stack | solution.py:103
  75.2 5.4 %all-to-all-start.1 = ((bf16[4,1536,512]{1,2,0:T(8,128)(2,1)}), bf16[4,1536,512]{1,2,0:T(8,128)(2,1)}, u32[]{:S(2)}, u32[]{:S(2)}) async-start(bf16[4,1536,512]{1,2,0:T(8,128)(2,1)} %stack.3), calls=%async_computation.1 | async-start | bytes 12582912 | tf_op jit(solution)/shard_map/all_to_all | solution.py:103
  81.5 85.7 %all-to-all-done.1 = bf16[4,1536,512]{1,2,0:T(8,128)(2,1)} async-done(((bf16[4,1536,512]{1,2,0:T(8,128)(2,1)}), bf16[4,1536,512]{1,2,0:T(8,128)(2,1)}, u32[]{:S(2)}, u32[]{:S(2)}) %all-to-all-start.1) | async-done | bytes 6291488 | tf_op jit(solution)/shard_map/all_to_all | solution.py:103
  167.2 3.7 %convert_reduce_fusion = f32[1536]{0:T(1024)S(1)} fusion(bf16[4,1536,512]{1,2,0:T(8,128)(2,1)} %all-to-all-done.1), kind=kLoop, calls=%fused_computation.4 | loop fusion | flops 6289920 | bytes 6297600 | tf_op jit(solution)/shard_map/reduce_sum | solution.py:28
  170.9 4.5 %fusion.2 = f32[1536]{0:T(1024)S(1)} fusion(bf16[4,1536,512]{1,2,0:T(8,128)(2,1)} %all-to-all-done.1, f32[1536]{0:T(1024)S(1)} %broadcast_multiply_fusion), kind=kLoop, calls=%fused_computation.7 | loop fusion | flops 12581376 | bytes 6303744 | tf_op jit(solution)/shard_map/reduce_sum | solution.py:29
  175.4 4.7 %fusion.4 = bf16[4,1536,512]{1,2,0:T(8,128)(2,1)S(1)} fusion(bf16[4,1536,512]{1,2,0:T(8,128)(2,1)} %all-to-all-done.1, f32[4,512]{1,0:T(4,128)S(1)} %mul.114, f32[1536]{0:T(1024)S(1)} %add_rsqrt_fusion, f32[1536]{0:T(1024)S(1)} %broadcast_multiply_fusion), kind=kLoop, calls=%fused_computation.9 | loop fusion | flops 15728640 | bytes 12603392 | tf_op jit(solution)/shard_map/convert.1
  180.0 3.5 %convolution_bitcast_fusion.1 = f32[512,1536]{0,1:T(8,128)S(1)} fusion(bf16[1536,2048]{0,1:T(8,128)(2,1)S(1)} %bitcast.51, bf16[1,2048,512]{2,1,0:T(8,128)(2,1)S(1)} %copy-done), kind=kOutput, calls=%fused_computation.19 | convolution fusion | flops 3221225472 | bytes 11534336 | tf_op jit(solution)/shard_map/dot_general | solution.py:113
  183.6 4.9 %fusion.11 = bf16[512,1536]{0,1:T(8,128)(2,1)} fusion(bf16[1536,2048]{0,1:T(8,128)(2,1)S(1)} %bitcast.52, f32[512,1536]{0,1:T(8,128)S(1)} %convolution_bitcast_fusion.1, bf16[1,2048,512]{2,1,0:T(8,128)(2,1)S(1)} %copy-done.6), kind=kOutput, calls=%fused_computation.20 | convolution fusion | flops 3225944064 | bytes 13107200 | tf_op jit(solution)/shard_map/dot_general | solution.py:116
  188.7 2.1 convert_reduce_fusion.1
  190.8 0.7 fusion.7
  191.6 1.3 fusion.23
  192.9 1.3 collective-permute-start
  194.2 1.5 collective-permute-start.1
  195.8 1.5 collective-permute-done.1
  197.4 3.3 %fusion.30 = bf16[512,512]{0,1:T(8,128)(2,1)} fusion(bf16[512,512]{0,1:T(8,128)(2,1)S(1)} %fusion.23, f32[512,528]{0,1:T(8,128)S(1)} %maximum_convert_fusion, f32[512]{0:T(512)S(1)} %copy-done.5, f32[512]{0:T(512)S(1)} %get-tuple-element.4, f32[512]{0:T(512)S(1)} %get-tuple-element.5, f32[512]{0:T(512)S(1)} %get-tuple-element.6, ...), kind=kLoop, calls=%fused_computation.53 | loop fusion | flops 7077888 | bytes 17838080 | tf_op jit(solution)/shard_map/convert_element_type | solution.py:55
  200.8 56.3 %all-gather.8.cloned.1.call-done = bf16[2048,1536]{0,1:T(8,128)(2,1)} async-done(((bf16[512,1536]{0,1:T(8,128)(2,1)}), bf16[2048,1536]{0,1:T(8,128)(2,1)}) %all-gather.8.cloned.1.call-update) | async-done | bytes 6291472 | tf_op jit(solution)/shard_map/all_gather | solution.py:129
  257.1 8.1 %convolution_convert_fusion = bf16[1536,512]{1,0:T(8,128)(2,1)} fusion(bf16[2048,1536]{0,1:T(8,128)(2,1)} %all-gather.8.cloned.1.call-done, bf16[1,2048,512]{2,1,0:T(8,128)(2,1)} %param.21), kind=kOutput, calls=%fused_computation.21 | convolution fusion | flops 3222011904 | bytes 9961472 | tf_op jit(solution)/shard_map/dot_general | solution.py:128
  265.2 4.7 %all-to-all-start.2 = ((bf16[8,192,512]{2,1,0:T(8,128)(2,1)}), bf16[8,192,512]{2,1,0:T(8,128)(2,1)}, u32[]{:S(2)}, u32[]{:S(2)}) async-start(bf16[8,192,512]{2,1,0:T(8,128)(2,1)} %bitcast.53), calls=%async_computation.2 | async-start | bytes 3145728 | tf_op jit(solution)/shard_map/all_to_all | solution.py:136
  270.1 24.5 %all-gather.6.cloned.1.call-done = bf16[2048,512]{0,1:T(8,128)(2,1)} async-done(((bf16[512,512]{0,1:T(8,128)(2,1)}), bf16[2048,512]{0,1:T(8,128)(2,1)}) %all-gather.6.cloned.1.call-update) | async-done | bytes 2097168 | tf_op jit(solution)/shard_map/all_gather | solution.py:123
  294.6 4.3 %convolution_convert_fusion.1 = bf16[512,512]{1,0:T(8,128)(2,1)} fusion(bf16[2048,512]{0,1:T(8,128)(2,1)} %all-gather.6.cloned.1.call-done, bf16[2048,512]{1,0:T(8,128)(2,1)} %param.17), kind=kOutput, calls=%fused_computation.32 | convolution fusion | flops 1074003968 | bytes 4718592 | tf_op jit(solution)/shard_map/dot_general | solution.py:122
  298.8 9.0 %all-to-all-done.2 = bf16[8,192,512]{2,1,0:T(8,128)(2,1)} async-done(((bf16[8,192,512]{2,1,0:T(8,128)(2,1)}), bf16[8,192,512]{2,1,0:T(8,128)(2,1)}, u32[]{:S(2)}, u32[]{:S(2)}) %all-to-all-start.2) | async-done | bytes 1572896 | tf_op jit(solution)/shard_map/all_to_all | solution.py:136
  307.8 5.6 %gather_fusion.1 = bf16[1024,512]{1,0:T(8,128)(2,1)S(1)} fusion(bf16[1536,512]{1,0:T(8,128)(2,1)} %bitcast.15, s32[1024]{0:T(1024)S(1)} %broadcast_clamp_fusion), kind=kCustom, calls=%fused_computation.1 | custom fusion | bytes 2101248 | tf_op jit(solution)/shard_map/gather | solution.py:139
  313.4 2.4 reshape.204
  315.8 5.2 %multiply_reduce_fusion = bf16[512,512]{1,0:T(8,128)(2,1)} fusion(f32[512,2,512]{2,1,0:T(2,128)} %reshape.204, f32[512,2]{1,0:T(8,128)S(1)} %copy.19), kind=kLoop, calls=%fused_computation.26 | loop fusion | flops 786432 | bytes 2625536 | tf_op jit(solution)/shard_map/reduce_sum | solution.py:140
  (54 shorter events, 2.9 us)
Async XLA Ops:
  7.2 172.9 %copy-start = (bf16[1,2048,512]{2,1,0:T(8,128)(2,1)S(1)}, bf16[1,2048,512]{2,1,0:T(8,128)(2,1)}, u32[]{:S(2)}) copy-start(bf16[1,2048,512]{2,1,0:T(8,128)(2,1)} %param.19) | copy-start | bytes 6291460
  7.2 9.7 %copy-start.1 = (bf16[512,512]{1,0:T(8,128)(2,1)S(1)}, bf16[512,512]{1,0:T(8,128)(2,1)}, u32[]{:S(2)}) copy-start(bf16[512,512]{1,0:T(8,128)(2,1)} %param.13) | copy-start | bytes 1572868
  75.2 6.3 %copy-start.3 = (f32[2048]{0:T(1024)S(1)}, f32[2048]{0:T(1024)}, u32[]{:S(2)}) copy-start(f32[2048]{0:T(1024)} %param.18) | copy-start | bytes 24580
  75.2 92.0 %all-to-all-start.1 = ((bf16[4,1536,512]{1,2,0:T(8,128)(2,1)}), bf16[4,1536,512]{1,2,0:T(8,128)(2,1)}, u32[]{:S(2)}, u32[]{:S(2)}) async-start(bf16[4,1536,512]{1,2,0:T(8,128)(2,1)} %stack.3), calls=%async_computation.1 | async-start | bytes 12582912 | tf_op jit(solution)/shard_map/all_to_all | solution.py:103
  80.5 108.1 %all-gather.4.cloned.1.call-start = ((), (), s32[]{:S(2)}) async-start(), calls=%async_computation.3 | async-start | bytes 2621440 | tf_op jit(solution)/shard_map/all_gather | solution.py:90
  81.3 175.8 %all-gather.8.cloned.1.call-start = ((), (), s32[]{:S(2)}) async-start(), calls=%async_computation.5 | async-start | bytes 7864320 | tf_op jit(solution)/shard_map/all_gather | solution.py:129
  180.0 3.5 %copy-start.6 = (bf16[1,2048,512]{2,1,0:T(8,128)(2,1)S(1)}, bf16[1,2048,512]{2,1,0:T(8,128)(2,1)}, u32[]{:S(2)}) copy-start(bf16[1,2048,512]{2,1,0:T(8,128)(2,1)} %param.20) | copy-start | bytes 6291460
  188.5 106.1 %all-gather.6.cloned.1.call-start = ((), (), s32[]{:S(2)}) async-start(), calls=%async_computation.4 | async-start | bytes 2621440 | tf_op jit(solution)/shard_map/all_gather | solution.py:123
  188.6 2.2 copy-start.2
  188.6 2.9 copy-start.7
  188.6 2.9 copy-start.8
  191.6 5.9 %copy-start.5 = (f32[512]{0:T(512)S(1)}, f32[512]{0:T(512)}, u32[]{:S(2)}) copy-start(f32[512]{0:T(512)} %param.15) | copy-start | bytes 6148
  192.9 2.8 collective-permute-start
  194.2 3.1 collective-permute-start.1
  265.2 4.7 %copy-start.4 = (f32[512,2]{0,1:T(2,128)S(1)}, f32[512,2]{0,1:T(2,128)}, u32[]{:S(2)}) copy-start(f32[512,2]{0,1:T(2,128)} %param.23) | copy-start | bytes 12292
  265.2 42.6 %all-to-all-start.2 = ((bf16[8,192,512]{2,1,0:T(8,128)(2,1)}), bf16[8,192,512]{2,1,0:T(8,128)(2,1)}, u32[]{:S(2)}, u32[]{:S(2)}) async-start(bf16[8,192,512]{2,1,0:T(8,128)(2,1)} %bitcast.53), calls=%async_computation.2 | async-start | bytes 3145728 | tf_op jit(solution)/shard_map/all_to_all | solution.py:136
Sparse Core Ops, SparseCore 0:
  83.2 73.4 all-gather.3
  188.6 68.4 all-gather.7
  259.5 35.0 all-gather.5
